TPU v7x, 32 devices: a whole 2x2x4 slice. The times are simulated.
32 devices in a mesh: ra: 2 (over core), cb: 4 (over z), dp: 4 (over y, x).
Axes of the slice: x: 2, y: 2, z: 4, core: 2. Of those that a mesh axis runs over, the one named last changes fastest.
Arguments:
- residual_in: bfloat16 [1024, 4096], P('dp', 'cb'), may hold values from -220 to 220, as said below
- gain_in: float32 [4096], P('cb'), may hold values from 0.1 to 1.9
- shift_in: float32 [4096], P('cb'), may hold values from -3 to 3
- up_weight: bfloat16 [4096, 16384], P('cb', 'ra'), may hold values from -0.09375 to 0.09375
- down_weight: bfloat16 [16384, 4096], P('ra', 'cb'), may hold values from -0.046875 to 0.046875
- gain_out: float32 [4096], P('cb'), may hold values from 0.1 to 1.9
- shift_out: float32 [4096], P('cb'), may hold values from -3 to 3
Outputs:
- layer_out: bfloat16 [1024, 4096], P('dp', 'cb')
Inputs may be any that keep to these rules, and one draw needn't show every extreme that they name: `residual_in`: real-valued activations.
All inputs are finite; a program needn't handle non-finite values.
Results may differ from a plain program's by a relative error of at most 0.0065.
Values may be sent and summed in bfloat16 or wider, within the bound.
No kernel may reach another device: no remote copies, remote signals or barrier semaphores. Data moves between devices by JAX's collectives and lax.ppermute only.
A program may use at most 128 MiB of HBM per device.

v0:
```python
import jax
import jax.numpy as jnp
from jax import lax
from jax.sharding import PartitionSpec as P


def standardize(values):
    count = values.shape[1] * lax.axis_size("cb")
    sums = lax.psum(jnp.sum(values, axis=1), "cb")
    mean = sums / count
    centred = values - mean[:, None]
    spread = lax.psum(jnp.sum(centred * centred, axis=1), "cb") / count
    return (values - mean[:, None]) * lax.rsqrt(spread + 1e-05)[:, None]


def per_device(residual_in, gain_in, shift_in, up_weight, down_weight, gain_out, shift_out):
    normed = (standardize(residual_in.astype(jnp.float32)) * gain_in + shift_in).astype(
        jnp.bfloat16
    )
    products = jnp.dot(normed, up_weight, preferred_element_type=jnp.float32)
    share = lax.psum_scatter(products, "cb", scatter_dimension=1, tiled=True)
    hidden_share = jnp.square(jax.nn.relu(share)).astype(jnp.bfloat16)
    branch_part = jnp.dot(
        lax.all_gather(hidden_share, "cb", axis=1, tiled=True),
        down_weight,
        preferred_element_type=jnp.float32,
    )
    branch = lax.psum(branch_part, "ra")
    total = 2.0**0.25 * normed.astype(jnp.float32) + branch
    return (standardize(total) * gain_out + shift_out).astype(jnp.bfloat16)


def solution(mesh):
    in_specs = (P("dp", "cb"), P("cb"), P("cb"), P("cb", "ra"), P("ra", "cb"), P("cb"), P("cb"))
    out_specs = P("dp", "cb")
    return jax.shard_map(
        per_device, mesh=mesh, in_specs=in_specs, out_specs=out_specs, check_vma=False
    )
```

profile of v0, /device:TPU:0, one launch (start us, length us, event | category | flops | bytes accessed | tf_op | source)
XLA Modules:
  0.0 337.2 jit_solution(11542523909155165681)
XLA Ops:
  6.5 1.2 convert_reduce_fusion
  7.7 13.5 %psum.35 = f32[256]{0:T(256)S(1)} all-reduce(f32[256]{0:T(256)S(1)} %convert_reduce_fusion), channel_id=1, replica_groups=mesh['ra'=2,'cb'=4,'dp'=4] {'cb'}, use_global_device_ids=true, to_apply=%region_1.0 | all-reduce | flops 256 | bytes 2048 | tf_op jit(solution)/shard_map/psum | solution.py:9
  21.2 1.3 fusion.2
  22.5 8.4 %psum.36 = f32[256]{0:T(256)S(1)} all-reduce(f32[256]{0:T(256)S(1)} %fusion.2), channel_id=1, replica_groups=mesh['ra'=2,'cb'=4,'dp'=4] {'cb'}, use_global_device_ids=true, to_apply=%region_3.0 | all-reduce | flops 256 | bytes 2048 | tf_op jit(solution)/shard_map/psum | solution.py:12
  30.9 13.8 %fusion.7 = f32[256,8192]{1,0:T(8,128)} fusion(bf16[1024,8192]{1,0:T(8,128)(2,1)} %param.10, bf16[256,1024]{1,0:T(8,128)(2,1)} %param.7, f32[1024]{0:T(1024)} %param.9, f32[1024]{0:T(1024)} %param.8, f32[256]{0:T(256)S(1)} %add_rsqrt_fusion.1, f32[256]{0:T(256)S(1)} %broadcast_multiply_fusion.1), kind=kOutput, calls=%fused_computation.17 | convolution fusion | flops 4296540160 | bytes 25700352 | tf_op jit(solution)/shard_map/dot_general | solution.py:20
  44.8 0.0 reduce-scatter.2.cloned.1.call-update
  44.8 0.0 all-gather.2.cloned.1.call-start
  44.8 144.4 %reduce-scatter.2.cloned.1.call-done = f32[256,2048]{1,0:T(8,128)} async-done(((f32[256,8192]{1,0:T(8,128)}), f32[256,2048]{1,0:T(8,128)}) %reduce-scatter.2.cloned.1.call-update) | async-done | bytes 2097168 | tf_op jit(solution)/shard_map/reduce_scatter | solution.py:21
  189.2 2.8 multiply_convert_fusion
  192.0 0.0 all-gather.2.cloned.1.call-update
  192.0 0.0 copy-start
  192.0 0.0 copy-start.1
  192.1 0.0 copy-start.2
  192.1 0.0 copy-start.3
  192.1 0.0 all-reduce.2.cloned.1.call-start
  192.1 81.4 %all-gather.2.cloned.1.call-done = bf16[256,8192]{1,0:T(8,128)(2,1)} async-done(((bf16[256,2048]{1,0:T(8,128)(2,1)}), bf16[256,8192]{1,0:T(8,128)(2,1)}) %all-gather.2.cloned.1.call-update) | async-done | bytes 4194320 | tf_op jit(solution)/shard_map/all_gather | solution.py:24
  273.5 12.5 %fusion.9 = f32[256,1024]{1,0:T(8,128)} fusion(bf16[256,8192]{1,0:T(8,128)(2,1)} %all-gather.2.cloned.1.call-done, bf16[8192,1024]{1,0:T(8,128)(2,1)} %param.11), kind=kOutput, calls=%fused_computation.18 | convolution fusion | flops 4294967296 | bytes 22020096 | tf_op jit(solution)/shard_map/dot_general | solution.py:23
  286.0 0.0 all-reduce.2.cloned.1.call-update
  286.1 18.1 %all-reduce.2.cloned.1.call-done = f32[256,1024]{1,0:T(8,128)} async-done(((f32[256,1024]{1,0:T(8,128)}), f32[256,1024]{1,0:T(8,128)}) %all-reduce.2.cloned.1.call-update) | async-done | bytes 1048592 | tf_op jit(solution)/shard_map/psum | solution.py:28
  304.1 1.7 fusion.6
  305.8 12.0 %psum.38 = f32[256]{0:T(256)S(1)} all-reduce(f32[256]{0:T(256)S(1)} %fusion.6), channel_id=1, replica_groups=mesh['ra'=2,'cb'=4,'dp'=4] {'cb'}, use_global_device_ids=true, to_apply=%region_7.8 | all-reduce | flops 256 | bytes 2048 | tf_op jit(solution)/shard_map/psum | solution.py:9
  317.8 1.7 multiply_reduce_fusion
  319.5 8.4 %psum.39 = f32[256]{0:T(256)S(1)} all-reduce(f32[256]{0:T(256)S(1)} %multiply_reduce_fusion), channel_id=1, replica_groups=mesh['ra'=2,'cb'=4,'dp'=4] {'cb'}, use_global_device_ids=true, to_apply=%region_9.10 | all-reduce | flops 256 | bytes 2048 | tf_op jit(solution)/shard_map/psum | solution.py:12
  327.9 2.8 add_convert_fusion
  (11 shorter events, 0.0 us)
Async XLA Ops:
  6.5 182.7 %reduce-scatter.2.cloned.1.call-start = ((), (), s32[]{:S(2)}) async-start(), calls=%async_computation.1 | async-start | bytes 10485760 | tf_op jit(solution)/shard_map/reduce_scatter | solution.py:21
  44.8 228.8 %all-gather.2.cloned.1.call-start = ((), (), s32[]{:S(2)}) async-start(), calls=%async_computation.2 | async-start | bytes 5242880 | tf_op jit(solution)/shard_map/all_gather | solution.py:24
  192.0 112.1 %copy-start = (bf16[256,1024]{1,0:T(8,128)(2,1)S(1)}, bf16[256,1024]{1,0:T(8,128)(2,1)}, u32[]{:S(2)}) copy-start(bf16[256,1024]{1,0:T(8,128)(2,1)} %param.7) | copy-start | bytes 1572868
  192.0 112.1 %copy-start.1 = (f32[1024]{0:T(1024)S(1)}, f32[1024]{0:T(1024)}, u32[]{:S(2)}) copy-start(f32[1024]{0:T(1024)} %param.9) | copy-start | bytes 12292
  192.1 112.1 %copy-start.2 = (f32[1024]{0:T(1024)S(1)}, f32[1024]{0:T(1024)}, u32[]{:S(2)}) copy-start(f32[1024]{0:T(1024)} %param.8) | copy-start | bytes 12292
  192.1 135.8 %copy-start.3 = (f32[1024]{0:T(1024)S(1)}, f32[1024]{0:T(1024)}, u32[]{:S(2)}) copy-start(f32[1024]{0:T(1024)} %param.13) | copy-start | bytes 12292
  192.1 135.8 %copy-start.4 = (f32[1024]{0:T(1024)S(1)}, f32[1024]{0:T(1024)}, u32[]{:S(2)}) copy-start(f32[1024]{0:T(1024)} %param.12) | copy-start | bytes 12292
  192.1 112.0 %all-reduce.2.cloned.1.call-start = ((), (), s32[]{:S(2)}) async-start(), calls=%async_computation.3 | async-start | bytes 2097152 | tf_op jit(solution)/shard_map/psum | solution.py:28
Sparse Core Ops, SparseCore 0:
  44.9 144.2 reduce-scatter.1
  192.2 81.3 all-gather.1
  286.2 17.8 all-reduce.1
where the time goes:
time: 338 us; the launch traced here: 337 us
  waiting for transfers between devices  244 us (72%)
  blocking collectives  42.2 us (12%)
  matrix products  26.3 us (8%)
  between operations  13.2 us (4%)
  other arithmetic  11.5 us (3%)
    reduce_scatter x1, waiting for transfers between devices, per_device(): share = lax.psum_scatter(products, 'cb', scatter_dimension=1, tiled=True)  144 us
    all_gather x1, waiting for transfers between devices, per_device(): lax.all_gather(hidden_share, 'cb', axis=1, tiled=True)  81.4 us
    psum x2, blocking collectives, standardize(): sums = lax.psum(jnp.sum(values, axis=1), 'cb')  25.5 us
    psum x1, waiting for transfers between devices, per_device(): branch = lax.psum(branch_part, 'ra')  18.1 us
    psum x2, blocking collectives, standardize(): spread = lax.psum(jnp.sum(centred * centred, axis=1), 'cb') / count  16.7 us
    dot_general x1, matrix products, per_device(): products = jnp.dot(normed, up_weight, preferred_element_type=jnp.float32)  13.8 us
    dot_general x1, matrix products, per_device(): jnp.dot(lax.all_gather(hidden_share, 'cb', axis=1, tiled=True), down_weig...  12.5 us
  transfers between devices with their start and end apart: 3, of which 3 were waited for; matrix products, arithmetic and copies ran while one was open for 0% of the time, Pallas kernels for 0%

commit v1 on v0

v1 whole, which is shorter than its diff:
```python
import jax
import jax.numpy as jnp
from jax import lax
from jax.sharding import PartitionSpec as P

PIECES = 16
LAG = 3
EPS = 1e-05


def gathered(values, axis):
    devices = lax.axis_size(axis)
    if devices > 4:
        return lax.all_gather(values, axis)
    shifts = [[(i, (i + by) % devices) for i in range(devices)] for by in range(1, devices)]
    return jnp.stack([values] + [lax.ppermute(values, axis, pairs) for pairs in shifts])


def row_statistics(values, axis):
    devices = lax.axis_size(axis)
    width = values.shape[1]
    mean = jnp.sum(values, axis=1) / width
    centred = values - mean[:, None]
    squares = jnp.sum(centred * centred, axis=1)
    both = gathered(jnp.stack([mean, squares]), axis)
    means = both[:, 0]
    whole_mean = jnp.mean(means, axis=0)
    offsets = means - whole_mean
    whole_squares = jnp.sum(both[:, 1], axis=0) + width * jnp.sum(offsets * offsets, axis=0)
    return whole_mean, whole_squares / (width * devices)


def layer_norm(values, gain, shift):
    mean, spread = row_statistics(values, "cb")
    return (values - mean[:, None]) * lax.rsqrt(spread + EPS)[:, None] * gain + shift


def activate(pre):
    return jnp.square(jax.nn.relu(pre)).astype(jnp.bfloat16)


def feed_forward_line(normed, up_weight, down_weight):
    place = lax.axis_index("cb")
    at_end = jnp.logical_or(place == 0, place == 3)
    inwards, outwards = [(0, 1), (3, 2)], [(1, 0), (2, 3)]
    piece = up_weight.shape[1] // PIECES
    cuts = [slice(at * piece, (at + 1) * piece) for at in range(PIECES)]
    hidden = {}
    branch = 0.0
    for step in range(PIECES + LAG):
        done = step - LAG
        if step < PIECES:
            part = jnp.dot(normed, up_weight[:, cuts[step]], preferred_element_type=jnp.float32)
        if done < 0:
            got = lax.ppermute(part.astype(jnp.bfloat16), "cb", inwards)
        elif step < PIECES:
            sent = jnp.where(at_end, part.astype(jnp.bfloat16), hidden[done])
            got = lax.ppermute(sent, "cb", inwards + outwards)
        else:
            got = lax.ppermute(hidden[done], "cb", outwards)
        if step < PIECES:
            half = part + got.astype(jnp.float32)
            other = lax.ppermute(half.astype(jnp.bfloat16), "cb", [(1, 2), (2, 1)])
            hidden[step] = activate(half + other.astype(jnp.float32))
        if done >= 0:
            whole = jnp.where(at_end, got, hidden[done])
            branch = branch + jnp.dot(
                whole, down_weight[cuts[done]], preferred_element_type=jnp.float32
            )
    return branch


def feed_forward_any(normed, up_weight, down_weight):
    products = jnp.dot(normed, up_weight, preferred_element_type=jnp.float32)
    share = lax.psum_scatter(products, "cb", scatter_dimension=1, tiled=True)
    hidden = lax.all_gather(activate(share), "cb", axis=1, tiled=True)
    return jnp.dot(hidden, down_weight, preferred_element_type=jnp.float32)


def per_device(residual_in, gain_in, shift_in, up_weight, down_weight, gain_out, shift_out):
    normed = layer_norm(residual_in.astype(jnp.float32), gain_in, shift_in).astype(jnp.bfloat16)
    normed = lax.optimization_barrier(normed)
    if lax.axis_size("cb") == 4 and up_weight.shape[1] % PIECES == 0:
        branch_part = feed_forward_line(normed, up_weight, down_weight)
    else:
        branch_part = feed_forward_any(normed, up_weight, down_weight)
    if lax.axis_size("ra") == 2:
        branch = branch_part + lax.ppermute(branch_part, "ra", [(0, 1), (1, 0)])
    else:
        branch = lax.psum(branch_part, "ra")
    total = 2.0**0.25 * normed.astype(jnp.float32) + branch
    return layer_norm(total, gain_out, shift_out).astype(jnp.bfloat16)


def solution(mesh):
    in_specs = (P("dp", "cb"), P("cb"), P("cb"), P("cb", "ra"), P("ra", "cb"), P("cb"), P("cb"))
    out_specs = P("dp", "cb")
    return jax.shard_map(
        per_device, mesh=mesh, in_specs=in_specs, out_specs=out_specs, check_vma=False
    )
```

time: 338 us -> 176 us (0.52)
  waiting for transfers between devices: 244 us -> 56.7 us
  starting transfers between devices: 0.09 us -> 82.6 us
  blocking collectives: 42.2 us -> 0 us
  between operations: 13.2 us -> 0.85 us
    reduce_scatter x1 -> x0, waiting for transfers between devices: 144 us -> none  [per_device(): share = lax.psum_scatter(products, 'cb', scatter_dimension=1, tiled=True)]
    ppermute x0 -> x42, starting transfers between devices: none -> 82.6 us  [the longest x13 50.9 us: feed_forward_line(): got = lax.ppermute(sent, 'cb', inwards + outwards)]
    all_gather x1 -> x0, waiting for transfers between devices: 81.4 us -> none  [per_device(): lax.all_gather(hidden_share, 'cb', axis=1, tiled=True)]
    ppermute x0 -> x42, waiting for transfers between devices: none -> 56.7 us  [the longest x13 26.5 us: feed_forward_line(): got = lax.ppermute(sent, 'cb', inwards + outwards)]
    psum x4 -> x0, blocking collectives: 42.2 us -> none  [the longest x2 25.5 us: standardize(): sums = lax.psum(jnp.sum(values, axis=1), 'cb')]
    psum x1 -> x0, waiting for transfers between devices: 18.1 us -> none  [per_device(): branch = lax.psum(branch_part, 'ra')]
    dot_general x2 -> x32, matrix products: 26.3 us -> 25.2 us  [the longest x16 17.5 us: feed_forward_line(): jnp.dot(normed, up_weight[:, cuts[step]], preferred_element_type=jnp.floa...]
  transfers between devices with their start and end apart: 3 -> 42, of which waited for: 3 -> 24; matrix products, arithmetic and copies ran while one was open for 0% -> 6% of each run, Pallas kernels for 0% -> 0%
where the time goes in v1:
time: 176 us; the launch traced here: 175 us
  starting transfers between devices  82.6 us (47%)
  waiting for transfers between devices  56.7 us (32%)
  matrix products  25.2 us (14%)
  other arithmetic  9.99 us (6%)
    ppermute x13, starting transfers between devices, feed_forward_line(): got = lax.ppermute(sent, 'cb', inwards + outwards)  50.9 us
    ppermute x13, waiting for transfers between devices, feed_forward_line(): got = lax.ppermute(sent, 'cb', inwards + outwards)  26.5 us
    dot_general x16, matrix products, feed_forward_line(): jnp.dot(normed, up_weight[:, cuts[step]], preferred_element_type=jnp.floa...  17.5 us
    ppermute x3, waiting for transfers between devices, feed_forward_line(): got = lax.ppermute(hidden[done], 'cb', outwards)  13 us
    ppermute x6, starting transfers between devices, gathered(): lax.ppermute(values, axis, pairs)  12.2 us
    ppermute x16, starting transfers between devices, feed_forward_line(): other = lax.ppermute(half.astype(jnp.bfloat16), 'cb', [(1, 2), (2, 1)])  11.2 us
    ppermute x3, waiting for transfers between devices, feed_forward_line(): got = lax.ppermute(part.astype(jnp.bfloat16), 'cb', inwards)  10.8 us
    dot_general x16, matrix products, feed_forward_line(): jnp.dot(whole, down_weight[cuts[done]], preferred_element_type=jnp.float32)  7.76 us
  transfers between devices with their start and end apart: 42, of which 24 were waited for; matrix products, arithmetic and copies ran while one was open for 6% of the time, Pallas kernels for 0%

profile of v1, /device:TPU:0, one launch (start us, length us, event | category | flops | bytes accessed | tf_op | source)
XLA Modules:
  0.0 175.5 jit_solution(12050848166678813055)
XLA Ops:
  2.5 4.1 %collective-permute-start.1 = (f32[2,256]{1,0:T(2,128)S(1)}, f32[2,256]{1,0:T(2,128)S(1)}, u32[]{:S(2)}, u32[]{:S(2)}) collective-permute-start(f32[2,256]{1,0:T(2,128)S(1)} %get-tuple-element.40), channel_id=1, source_target_pairs={{0,8},{4,12},{8,0},{12,4},{1,9},{5,13},{9,1},{13,5},{2,10},{6,14},... | collective-permute-start | bytes 6152 | tf_op jit(solution)/shard_map/ppermute | solution.py:16
  36.3 3.6 %collective-permute-done.9 = bf16[256,512]{1,0:T(8,128)(2,1)S(1)} collective-permute-done((bf16[256,512]{1,0:T(8,128)(2,1)S(1)}, bf16[256,512]{1,0:T(8,128)(2,1)S(1)}, u32[]{:S(2)}, u32[]{:S(2)}) %collective-permute-start.9) | collective-permute-done | bytes 262176 | tf_op jit(solution)/shard_map/ppermute | solution.py:55
  40.6 4.9 %collective-permute-done.6 = bf16[256,512]{1,0:T(8,128)(2,1)S(1)} collective-permute-done((bf16[256,512]{1,0:T(8,128)(2,1)S(1)}, bf16[256,512]{1,0:T(8,128)(2,1)S(1)}, u32[]{:S(2)}, u32[]{:S(2)}) %collective-permute-start.6) | collective-permute-done | bytes 262176 | tf_op jit(solution)/shard_map/ppermute | solution.py:55
  49.7 5.7 %collective-permute-start.11 = (bf16[256,512]{1,0:T(8,128)(2,1)S(1)}, bf16[256,512]{1,0:T(8,128)(2,1)S(1)}, u32[]{:S(2)}, u32[]{:S(2)}) collective-permute-start(bf16[256,512]{1,0:T(8,128)(2,1)S(1)} %get-tuple-element.25), channel_id=1, source_target_pairs={{0,4},{12,8},{4,0},{8,12},{1,5},{13,9},{5,1},{9,13},{2,6},{14,10},... | collective-permute-start | bytes 786440 | tf_op jit(solution)/shard_map/ppermute | solution.py:58
  55.6 3.3 %collective-permute-start.8 = (bf16[256,512]{1,0:T(8,128)(2,1)S(1)}, bf16[256,512]{1,0:T(8,128)(2,1)S(1)}, u32[]{:S(2)}, u32[]{:S(2)}) collective-permute-start(bf16[256,512]{1,0:T(8,128)(2,1)S(1)} %get-tuple-element.17), channel_id=1, source_target_pairs={{0,4},{12,8},{4,0},{8,12},{1,5},{13,9},{5,1},{9,13},{2,6},{14,10},... | collective-permute-start | bytes 786440 | tf_op jit(solution)/shard_map/ppermute | solution.py:58
  59.1 3.1 %collective-permute-start.5 = (bf16[256,512]{1,0:T(8,128)(2,1)S(1)}, bf16[256,512]{1,0:T(8,128)(2,1)S(1)}, u32[]{:S(2)}, u32[]{:S(2)}) collective-permute-start(bf16[256,512]{1,0:T(8,128)(2,1)S(1)} %get-tuple-element.35), channel_id=1, source_target_pairs={{0,4},{12,8},{4,0},{8,12},{1,5},{13,9},{5,1},{9,13},{2,6},{14,10},... | collective-permute-start | bytes 786440 | tf_op jit(solution)/shard_map/ppermute | solution.py:58
  63.3 4.7 %collective-permute-done.8 = bf16[256,512]{1,0:T(8,128)(2,1)S(1)} collective-permute-done((bf16[256,512]{1,0:T(8,128)(2,1)S(1)}, bf16[256,512]{1,0:T(8,128)(2,1)S(1)}, u32[]{:S(2)}, u32[]{:S(2)}) %collective-permute-start.8) | collective-permute-done | bytes 262176 | tf_op jit(solution)/shard_map/ppermute | solution.py:58
  72.7 4.3 %collective-permute-start.17 = (bf16[256,512]{1,0:T(8,128)(2,1)S(1)}, bf16[256,512]{1,0:T(8,128)(2,1)S(1)}, u32[]{:S(2)}, u32[]{:S(2)}) collective-permute-start(bf16[256,512]{1,0:T(8,128)(2,1)S(1)} %get-tuple-element.23), channel_id=1, source_target_pairs={{0,4},{12,8},{4,0},{8,12},{1,5},{13,9},{5,1},{9,13},{2,6},{14,10},... | collective-permute-start | bytes 786440 | tf_op jit(solution)/shard_map/ppermute | solution.py:58
  77.2 2.7 %collective-permute-start.15 = (bf16[256,512]{1,0:T(8,128)(2,1)S(1)}, bf16[256,512]{1,0:T(8,128)(2,1)S(1)}, u32[]{:S(2)}, u32[]{:S(2)}) collective-permute-start(bf16[256,512]{1,0:T(8,128)(2,1)S(1)} %get-tuple-element.15), channel_id=1, source_target_pairs={{0,4},{12,8},{4,0},{8,12},{1,5},{13,9},{5,1},{9,13},{2,6},{14,10},... | collective-permute-start | bytes 786440 | tf_op jit(solution)/shard_map/ppermute | solution.py:58
  80.0 2.6 %collective-permute-start.13 = (bf16[256,512]{1,0:T(8,128)(2,1)S(1)}, bf16[256,512]{1,0:T(8,128)(2,1)S(1)}, u32[]{:S(2)}, u32[]{:S(2)}) collective-permute-start(bf16[256,512]{1,0:T(8,128)(2,1)S(1)} %get-tuple-element.33), channel_id=1, source_target_pairs={{0,4},{12,8},{4,0},{8,12},{1,5},{13,9},{5,1},{9,13},{2,6},{14,10},... | collective-permute-start | bytes 786440 | tf_op jit(solution)/shard_map/ppermute | solution.py:58
  84.9 2.9 %collective-permute-done.15 = bf16[256,512]{1,0:T(8,128)(2,1)S(1)} collective-permute-done((bf16[256,512]{1,0:T(8,128)(2,1)S(1)}, bf16[256,512]{1,0:T(8,128)(2,1)S(1)}, u32[]{:S(2)}, u32[]{:S(2)}) %collective-permute-start.15) | collective-permute-done | bytes 262176 | tf_op jit(solution)/shard_map/ppermute | solution.py:58
  93.0 4.5 %collective-permute-start.23 = (bf16[256,512]{1,0:T(8,128)(2,1)S(1)}, bf16[256,512]{1,0:T(8,128)(2,1)S(1)}, u32[]{:S(2)}, u32[]{:S(2)}) collective-permute-start(bf16[256,512]{1,0:T(8,128)(2,1)S(1)} %get-tuple-element.21), channel_id=1, source_target_pairs={{0,4},{12,8},{4,0},{8,12},{1,5},{13,9},{5,1},{9,13},{2,6},{14,10},... | collective-permute-start | bytes 786440 | tf_op jit(solution)/shard_map/ppermute | solution.py:58
  97.6 2.7 %collective-permute-start.21 = (bf16[256,512]{1,0:T(8,128)(2,1)S(1)}, bf16[256,512]{1,0:T(8,128)(2,1)S(1)}, u32[]{:S(2)}, u32[]{:S(2)}) collective-permute-start(bf16[256,512]{1,0:T(8,128)(2,1)S(1)} %get-tuple-element.13), channel_id=1, source_target_pairs={{0,4},{12,8},{4,0},{8,12},{1,5},{13,9},{5,1},{9,13},{2,6},{14,10},... | collective-permute-start | bytes 786440 | tf_op jit(solution)/shard_map/ppermute | solution.py:58
  100.5 2.6 %collective-permute-start.19 = (bf16[256,512]{1,0:T(8,128)(2,1)S(1)}, bf16[256,512]{1,0:T(8,128)(2,1)S(1)}, u32[]{:S(2)}, u32[]{:S(2)}) collective-permute-start(bf16[256,512]{1,0:T(8,128)(2,1)S(1)} %get-tuple-element.31), channel_id=1, source_target_pairs={{0,4},{12,8},{4,0},{8,12},{1,5},{13,9},{5,1},{9,13},{2,6},{14,10},... | collective-permute-start | bytes 786440 | tf_op jit(solution)/shard_map/ppermute | solution.py:58
  105.4 2.4 %collective-permute-done.21 = bf16[256,512]{1,0:T(8,128)(2,1)S(1)} collective-permute-done((bf16[256,512]{1,0:T(8,128)(2,1)S(1)}, bf16[256,512]{1,0:T(8,128)(2,1)S(1)}, u32[]{:S(2)}, u32[]{:S(2)}) %collective-permute-start.21) | collective-permute-done | bytes 262176 | tf_op jit(solution)/shard_map/ppermute | solution.py:58
  113.1 4.2 %collective-permute-start.29 = (bf16[256,512]{1,0:T(8,128)(2,1)S(1)}, bf16[256,512]{1,0:T(8,128)(2,1)S(1)}, u32[]{:S(2)}, u32[]{:S(2)}) collective-permute-start(bf16[256,512]{1,0:T(8,128)(2,1)S(1)} %get-tuple-element.19), channel_id=1, source_target_pairs={{0,4},{12,8},{4,0},{8,12},{1,5},{13,9},{5,1},{9,13},{2,6},{14,10},... | collective-permute-start | bytes 786440 | tf_op jit(solution)/shard_map/ppermute | solution.py:58
  117.6 2.6 %collective-permute-start.27 = (bf16[256,512]{1,0:T(8,128)(2,1)S(1)}, bf16[256,512]{1,0:T(8,128)(2,1)S(1)}, u32[]{:S(2)}, u32[]{:S(2)}) collective-permute-start(bf16[256,512]{1,0:T(8,128)(2,1)S(1)} %get-tuple-element.11), channel_id=1, source_target_pairs={{0,4},{12,8},{4,0},{8,12},{1,5},{13,9},{5,1},{9,13},{2,6},{14,10},... | collective-permute-start | bytes 786440 | tf_op jit(solution)/shard_map/ppermute | solution.py:58
  120.4 3.4 %collective-permute-start.25 = (bf16[256,512]{1,0:T(8,128)(2,1)S(1)}, bf16[256,512]{1,0:T(8,128)(2,1)S(1)}, u32[]{:S(2)}, u32[]{:S(2)}) collective-permute-start(bf16[256,512]{1,0:T(8,128)(2,1)S(1)} %get-tuple-element.29), channel_id=1, source_target_pairs={{0,4},{12,8},{4,0},{8,12},{1,5},{13,9},{5,1},{9,13},{2,6},{14,10},... | collective-permute-start | bytes 786440 | tf_op jit(solution)/shard_map/ppermute | solution.py:58
  131.9 9.1 %collective-permute-start.31 = (bf16[256,512]{1,0:T(8,128)(2,1)S(1)}, bf16[256,512]{1,0:T(8,128)(2,1)S(1)}, u32[]{:S(2)}, u32[]{:S(2)}) collective-permute-start(bf16[256,512]{1,0:T(8,128)(2,1)S(1)} %get-tuple-element.27), channel_id=1, source_target_pairs={{0,4},{12,8},{4,0},{8,12},{1,5},{13,9},{5,1},{9,13},{2,6},{14,10},... | collective-permute-start | bytes 786440 | tf_op jit(solution)/shard_map/ppermute | solution.py:58
  143.9 2.7 %collective-permute-done.31 = bf16[256,512]{1,0:T(8,128)(2,1)S(1)} collective-permute-done((bf16[256,512]{1,0:T(8,128)(2,1)S(1)}, bf16[256,512]{1,0:T(8,128)(2,1)S(1)}, u32[]{:S(2)}, u32[]{:S(2)}) %collective-permute-start.31) | collective-permute-done | bytes 262176 | tf_op jit(solution)/shard_map/ppermute | solution.py:58
  149.9 4.4 %collective-permute-done.33 = bf16[256,512]{1,0:T(8,128)(2,1)S(1)} collective-permute-done((bf16[256,512]{1,0:T(8,128)(2,1)S(1)}, bf16[256,512]{1,0:T(8,128)(2,1)S(1)}, u32[]{:S(2)}, u32[]{:S(2)}) %collective-permute-start.33) | collective-permute-done | bytes 262176 | tf_op jit(solution)/shard_map/ppermute | solution.py:60
  156.6 6.5 %collective-permute-done.37 = bf16[256,512]{1,0:T(8,128)(2,1)S(1)} collective-permute-done((bf16[256,512]{1,0:T(8,128)(2,1)S(1)}, bf16[256,512]{1,0:T(8,128)(2,1)S(1)}, u32[]{:S(2)}, u32[]{:S(2)}) %collective-permute-start.37) | collective-permute-done | bytes 262176 | tf_op jit(solution)/shard_map/ppermute | solution.py:60
  164.7 2.6 %collective-permute-done.38 = f32[256,1024]{1,0:T(8,128)S(1)} collective-permute-done((f32[256,1024]{1,0:T(8,128)S(1)}, f32[256,1024]{1,0:T(8,128)S(1)}, u32[]{:S(2)}, u32[]{:S(2)}) %collective-permute-start.38) | collective-permute-done | bytes 1048608 | tf_op jit(solution)/shard_map/ppermute | solution.py:88
  168.3 2.5 %collective-permute-start.39 = (f32[2,256]{1,0:T(2,128)S(1)}, f32[2,256]{1,0:T(2,128)S(1)}, u32[]{:S(2)}, u32[]{:S(2)}) collective-permute-start(f32[2,256]{1,0:T(2,128)S(1)} %get-tuple-element.38), channel_id=1, source_target_pairs={{0,4},{4,8},{8,12},{12,0},{1,5},{5,9},{9,13},{13,1},{2,6},{6,10},{... | collective-permute-start | bytes 6152 | tf_op jit(solution)/shard_map/ppermute | solution.py:16
  (167 shorter events, 82.4 us)
Async XLA Ops:
  33.2 12.3 %collective-permute-start.6 = (bf16[256,512]{1,0:T(8,128)(2,1)S(1)}, bf16[256,512]{1,0:T(8,128)(2,1)S(1)}, u32[]{:S(2)}, u32[]{:S(2)}) collective-permute-start(bf16[256,512]{1,0:T(8,128)(2,1)S(1)} %get-tuple-element.45), channel_id=1, source_target_pairs={{0,4},{12,8},{1,5},{13,9},{2,6},{14,10},{3,7},{15,11},{16,20},{28,... | collective-permute-start | bytes 786440 | tf_op jit(solution)/shard_map/ppermute | solution.py:55
  35.0 13.6 %collective-permute-start.3 = (bf16[256,512]{1,0:T(8,128)(2,1)S(1)}, bf16[256,512]{1,0:T(8,128)(2,1)S(1)}, u32[]{:S(2)}, u32[]{:S(2)}) collective-permute-start(bf16[256,512]{1,0:T(8,128)(2,1)S(1)} %get-tuple-element.41), channel_id=1, source_target_pairs={{0,4},{12,8},{1,5},{13,9},{2,6},{14,10},{3,7},{15,11},{16,20},{28,... | collective-permute-start | bytes 786440 | tf_op jit(solution)/shard_map/ppermute | solution.py:55
  39.9 9.6 %collective-permute-start.10 = (bf16[256,512]{1,0:T(8,128)(2,1)S(1)}, bf16[256,512]{1,0:T(8,128)(2,1)S(1)}, u32[]{:S(2)}, u32[]{:S(2)}) collective-permute-start(bf16[256,512]{1,0:T(8,128)(2,1)S(1)} %fusion.85), channel_id=1, source_target_pairs={{4,8},{8,4},{5,9},{9,5},{6,10},{10,6},{7,11},{11,7},{20,24},{24,20... | collective-permute-start | bytes 786440 | tf_op jit(solution)/shard_map/ppermute | solution.py:63
  45.5 9.8 %collective-permute-start.7 = (bf16[256,512]{1,0:T(8,128)(2,1)S(1)}, bf16[256,512]{1,0:T(8,128)(2,1)S(1)}, u32[]{:S(2)}, u32[]{:S(2)}) collective-permute-start(bf16[256,512]{1,0:T(8,128)(2,1)S(1)} %fusion.84), channel_id=1, source_target_pairs={{4,8},{8,4},{5,9},{9,5},{6,10},{10,6},{7,11},{11,7},{20,24},{24,20... | collective-permute-start | bytes 786440 | tf_op jit(solution)/shard_map/ppermute | solution.py:63
  48.7 10.2 %collective-permute-start.4 = (bf16[256,512]{1,0:T(8,128)(2,1)S(1)}, bf16[256,512]{1,0:T(8,128)(2,1)S(1)}, u32[]{:S(2)}, u32[]{:S(2)}) collective-permute-start(bf16[256,512]{1,0:T(8,128)(2,1)S(1)} %fusion.83), channel_id=1, source_target_pairs={{4,8},{8,4},{5,9},{9,5},{6,10},{10,6},{7,11},{11,7},{20,24},{24,20... | collective-permute-start | bytes 786440 | tf_op jit(solution)/shard_map/ppermute | solution.py:63
  49.7 12.8 %collective-permute-start.11 = (bf16[256,512]{1,0:T(8,128)(2,1)S(1)}, bf16[256,512]{1,0:T(8,128)(2,1)S(1)}, u32[]{:S(2)}, u32[]{:S(2)}) collective-permute-start(bf16[256,512]{1,0:T(8,128)(2,1)S(1)} %get-tuple-element.25), channel_id=1, source_target_pairs={{0,4},{12,8},{4,0},{8,12},{1,5},{13,9},{5,1},{9,13},{2,6},{14,10},... | collective-permute-start | bytes 786440 | tf_op jit(solution)/shard_map/ppermute | solution.py:58
  55.6 12.4 %collective-permute-start.8 = (bf16[256,512]{1,0:T(8,128)(2,1)S(1)}, bf16[256,512]{1,0:T(8,128)(2,1)S(1)}, u32[]{:S(2)}, u32[]{:S(2)}) collective-permute-start(bf16[256,512]{1,0:T(8,128)(2,1)S(1)} %get-tuple-element.17), channel_id=1, source_target_pairs={{0,4},{12,8},{4,0},{8,12},{1,5},{13,9},{5,1},{9,13},{2,6},{14,10},... | collective-permute-start | bytes 786440 | tf_op jit(solution)/shard_map/ppermute | solution.py:58
  59.1 11.8 %collective-permute-start.5 = (bf16[256,512]{1,0:T(8,128)(2,1)S(1)}, bf16[256,512]{1,0:T(8,128)(2,1)S(1)}, u32[]{:S(2)}, u32[]{:S(2)}) collective-permute-start(bf16[256,512]{1,0:T(8,128)(2,1)S(1)} %get-tuple-element.35), channel_id=1, source_target_pairs={{0,4},{12,8},{4,0},{8,12},{1,5},{13,9},{5,1},{9,13},{2,6},{14,10},... | collective-permute-start | bytes 786440 | tf_op jit(solution)/shard_map/ppermute | solution.py:58
  62.6 9.9 %collective-permute-start.16 = (bf16[256,512]{1,0:T(8,128)(2,1)S(1)}, bf16[256,512]{1,0:T(8,128)(2,1)S(1)}, u32[]{:S(2)}, u32[]{:S(2)}) collective-permute-start(bf16[256,512]{1,0:T(8,128)(2,1)S(1)} %fusion.88), channel_id=1, source_target_pairs={{4,8},{8,4},{5,9},{9,5},{6,10},{10,6},{7,11},{11,7},{20,24},{24,20... | collective-permute-start | bytes 786440 | tf_op jit(solution)/shard_map/ppermute | solution.py:63
  72.7 11.4 %collective-permute-start.17 = (bf16[256,512]{1,0:T(8,128)(2,1)S(1)}, bf16[256,512]{1,0:T(8,128)(2,1)S(1)}, u32[]{:S(2)}, u32[]{:S(2)}) collective-permute-start(bf16[256,512]{1,0:T(8,128)(2,1)S(1)} %get-tuple-element.23), channel_id=1, source_target_pairs={{0,4},{12,8},{4,0},{8,12},{1,5},{13,9},{5,1},{9,13},{2,6},{14,10},... | collective-permute-start | bytes 786440 | tf_op jit(solution)/shard_map/ppermute | solution.py:58
  77.2 10.7 %collective-permute-start.15 = (bf16[256,512]{1,0:T(8,128)(2,1)S(1)}, bf16[256,512]{1,0:T(8,128)(2,1)S(1)}, u32[]{:S(2)}, u32[]{:S(2)}) collective-permute-start(bf16[256,512]{1,0:T(8,128)(2,1)S(1)} %get-tuple-element.15), channel_id=1, source_target_pairs={{0,4},{12,8},{4,0},{8,12},{1,5},{13,9},{5,1},{9,13},{2,6},{14,10},... | collective-permute-start | bytes 786440 | tf_op jit(solution)/shard_map/ppermute | solution.py:58
  80.0 10.6 %collective-permute-start.13 = (bf16[256,512]{1,0:T(8,128)(2,1)S(1)}, bf16[256,512]{1,0:T(8,128)(2,1)S(1)}, u32[]{:S(2)}, u32[]{:S(2)}) collective-permute-start(bf16[256,512]{1,0:T(8,128)(2,1)S(1)} %get-tuple-element.33), channel_id=1, source_target_pairs={{0,4},{12,8},{4,0},{8,12},{1,5},{13,9},{5,1},{9,13},{2,6},{14,10},... | collective-permute-start | bytes 786440 | tf_op jit(solution)/shard_map/ppermute | solution.py:58
  87.9 9.6 %collective-permute-start.20 = (bf16[256,512]{1,0:T(8,128)(2,1)S(1)}, bf16[256,512]{1,0:T(8,128)(2,1)S(1)}, u32[]{:S(2)}, u32[]{:S(2)}) collective-permute-start(bf16[256,512]{1,0:T(8,128)(2,1)S(1)} %fusion.90), channel_id=1, source_target_pairs={{4,8},{8,4},{5,9},{9,5},{6,10},{10,6},{7,11},{11,7},{20,24},{24,20... | collective-permute-start | bytes 786440 | tf_op jit(solution)/shard_map/ppermute | solution.py:63
  90.7 9.7 %collective-permute-start.18 = (bf16[256,512]{1,0:T(8,128)(2,1)S(1)}, bf16[256,512]{1,0:T(8,128)(2,1)S(1)}, u32[]{:S(2)}, u32[]{:S(2)}) collective-permute-start(bf16[256,512]{1,0:T(8,128)(2,1)S(1)} %fusion.89), channel_id=1, source_target_pairs={{4,8},{8,4},{5,9},{9,5},{6,10},{10,6},{7,11},{11,7},{20,24},{24,20... | collective-permute-start | bytes 786440 | tf_op jit(solution)/shard_map/ppermute | solution.py:63
  93.0 11.6 %collective-permute-start.23 = (bf16[256,512]{1,0:T(8,128)(2,1)S(1)}, bf16[256,512]{1,0:T(8,128)(2,1)S(1)}, u32[]{:S(2)}, u32[]{:S(2)}) collective-permute-start(bf16[256,512]{1,0:T(8,128)(2,1)S(1)} %get-tuple-element.21), channel_id=1, source_target_pairs={{0,4},{12,8},{4,0},{8,12},{1,5},{13,9},{5,1},{9,13},{2,6},{14,10},... | collective-permute-start | bytes 786440 | tf_op jit(solution)/shard_map/ppermute | solution.py:58
  97.6 10.2 %collective-permute-start.21 = (bf16[256,512]{1,0:T(8,128)(2,1)S(1)}, bf16[256,512]{1,0:T(8,128)(2,1)S(1)}, u32[]{:S(2)}, u32[]{:S(2)}) collective-permute-start(bf16[256,512]{1,0:T(8,128)(2,1)S(1)} %get-tuple-element.13), channel_id=1, source_target_pairs={{0,4},{12,8},{4,0},{8,12},{1,5},{13,9},{5,1},{9,13},{2,6},{14,10},... | collective-permute-start | bytes 786440 | tf_op jit(solution)/shard_map/ppermute | solution.py:58
  100.5 10.1 %collective-permute-start.19 = (bf16[256,512]{1,0:T(8,128)(2,1)S(1)}, bf16[256,512]{1,0:T(8,128)(2,1)S(1)}, u32[]{:S(2)}, u32[]{:S(2)}) collective-permute-start(bf16[256,512]{1,0:T(8,128)(2,1)S(1)} %get-tuple-element.31), channel_id=1, source_target_pairs={{0,4},{12,8},{4,0},{8,12},{1,5},{13,9},{5,1},{9,13},{2,6},{14,10},... | collective-permute-start | bytes 786440 | tf_op jit(solution)/shard_map/ppermute | solution.py:58
  107.9 9.5 %collective-permute-start.26 = (bf16[256,512]{1,0:T(8,128)(2,1)S(1)}, bf16[256,512]{1,0:T(8,128)(2,1)S(1)}, u32[]{:S(2)}, u32[]{:S(2)}) collective-permute-start(bf16[256,512]{1,0:T(8,128)(2,1)S(1)} %fusion.93), channel_id=1, source_target_pairs={{4,8},{8,4},{5,9},{9,5},{6,10},{10,6},{7,11},{11,7},{20,24},{24,20... | collective-permute-start | bytes 786440 | tf_op jit(solution)/shard_map/ppermute | solution.py:63
  110.7 9.5 %collective-permute-start.24 = (bf16[256,512]{1,0:T(8,128)(2,1)S(1)}, bf16[256,512]{1,0:T(8,128)(2,1)S(1)}, u32[]{:S(2)}, u32[]{:S(2)}) collective-permute-start(bf16[256,512]{1,0:T(8,128)(2,1)S(1)} %fusion.92), channel_id=1, source_target_pairs={{4,8},{8,4},{5,9},{9,5},{6,10},{10,6},{7,11},{11,7},{20,24},{24,20... | collective-permute-start | bytes 786440 | tf_op jit(solution)/shard_map/ppermute | solution.py:63
  113.1 10.8 %collective-permute-start.29 = (bf16[256,512]{1,0:T(8,128)(2,1)S(1)}, bf16[256,512]{1,0:T(8,128)(2,1)S(1)}, u32[]{:S(2)}, u32[]{:S(2)}) collective-permute-start(bf16[256,512]{1,0:T(8,128)(2,1)S(1)} %get-tuple-element.19), channel_id=1, source_target_pairs={{0,4},{12,8},{4,0},{8,12},{1,5},{13,9},{5,1},{9,13},{2,6},{14,10},... | collective-permute-start | bytes 786440 | tf_op jit(solution)/shard_map/ppermute | solution.py:58
  124.1 17.0 %collective-permute-start.34 = (bf16[256,512]{1,0:T(8,128)(2,1)S(1)}, bf16[256,512]{1,0:T(8,128)(2,1)S(1)}, u32[]{:S(2)}, u32[]{:S(2)}) collective-permute-start(bf16[256,512]{1,0:T(8,128)(2,1)S(1)} %fusion.97), channel_id=1, source_target_pairs={{4,8},{8,4},{5,9},{9,5},{6,10},{10,6},{7,11},{11,7},{20,24},{24,20... | collective-permute-start | bytes 786440 | tf_op jit(solution)/shard_map/ppermute | solution.py:63
  126.9 15.6 %collective-permute-start.32 = (bf16[256,512]{1,0:T(8,128)(2,1)S(1)}, bf16[256,512]{1,0:T(8,128)(2,1)S(1)}, u32[]{:S(2)}, u32[]{:S(2)}) collective-permute-start(bf16[256,512]{1,0:T(8,128)(2,1)S(1)} %fusion.96), channel_id=1, source_target_pairs={{4,8},{8,4},{5,9},{9,5},{6,10},{10,6},{7,11},{11,7},{20,24},{24,20... | collective-permute-start | bytes 786440 | tf_op jit(solution)/shard_map/ppermute | solution.py:63
  131.9 14.6 %collective-permute-start.31 = (bf16[256,512]{1,0:T(8,128)(2,1)S(1)}, bf16[256,512]{1,0:T(8,128)(2,1)S(1)}, u32[]{:S(2)}, u32[]{:S(2)}) collective-permute-start(bf16[256,512]{1,0:T(8,128)(2,1)S(1)} %get-tuple-element.27), channel_id=1, source_target_pairs={{0,4},{12,8},{4,0},{8,12},{1,5},{13,9},{5,1},{9,13},{2,6},{14,10},... | collective-permute-start | bytes 786440 | tf_op jit(solution)/shard_map/ppermute | solution.py:58
  142.6 11.7 %collective-permute-start.33 = (bf16[256,512]{1,0:T(8,128)(2,1)S(1)}, bf16[256,512]{1,0:T(8,128)(2,1)S(1)}, u32[]{:S(2)}, u32[]{:S(2)}) collective-permute-start(bf16[256,512]{1,0:T(8,128)(2,1)S(1)} %multiply_convert_fusion.2), channel_id=1, source_target_pairs={{4,0},{8,12},{5,1},{9,13},{6,2},{10,14},{7,3},{11,15},{20,16},{24,... | collective-permute-start | bytes 786440 | tf_op jit(solution)/shard_map/ppermute | solution.py:60
  (25 other events, 339.9 us)

commit v2 on v1

v2 whole, which is shorter than its diff:
```python
import functools

import jax
import jax.numpy as jnp
from jax import lax
from jax.experimental import pallas as pl
from jax.experimental.pallas import tpu as pltpu
from jax.sharding import PartitionSpec as P

PIECES = 16
LAG = 4
MIB = 2**20
GROUPS = ((1, 3), (4, 6), (10, 6))
SMALL_GRANT = 8 * MIB
LARGE_GRANT = 50 * MIB
EPS = 1e-05


def gathered(values, axis):
    devices = lax.axis_size(axis)
    if devices > 4:
        return list(lax.all_gather(values, axis))
    shifts = [[(i, (i + by) % devices) for i in range(devices)] for by in range(1, devices)]
    return [values] + [lax.ppermute(values, axis, pairs) for pairs in shifts]


def row_statistics(values, axis):
    devices = lax.axis_size(axis)
    width = values.shape[1]
    mean = jnp.sum(values, axis=1) / width
    centred = values - mean[:, None]
    squares = jnp.sum(centred * centred, axis=1)
    both = jnp.stack(gathered(jnp.stack([mean, squares]), axis))
    means = both[:, 0]
    whole_mean = jnp.mean(means, axis=0)
    offsets = means - whole_mean
    whole_squares = jnp.sum(both[:, 1], axis=0) + width * jnp.sum(offsets * offsets, axis=0)
    return whole_mean, whole_squares / (width * devices)


def layer_norm(values, gain, shift):
    mean, spread = row_statistics(values, "cb")
    return (values - mean[:, None]) * lax.rsqrt(spread + EPS)[:, None] * gain + shift


def activate(pre):
    return jnp.square(jax.nn.relu(pre)).astype(jnp.bfloat16)


def columns_of(first, second):
    lane = lax.broadcasted_iota(jnp.int32, (first.shape[0], 128), 1)
    return jnp.where(lane == 0, first, second).T[:8]


def statistics_kernel(values_ref, out_ref, kept_ref):
    kept_ref[...] = values_ref[...]
    values = values_ref[...].astype(jnp.float32)
    mean = jnp.sum(values, axis=1, keepdims=True) / values.shape[1]
    centred = values - mean
    out_ref[...] = columns_of(mean, jnp.sum(centred * centred, axis=1, keepdims=True))


def statistics(values):
    whole = pl.BlockSpec(memory_space=pltpu.VMEM)
    return pl.pallas_call(
        statistics_kernel,
        in_specs=[whole],
        out_specs=[whole] * 2,
        out_shape=[
            jax.ShapeDtypeStruct((8, values.shape[0]), jnp.float32),
            jax.ShapeDtypeStruct(values.shape, values.dtype),
        ],
        compiler_params=pltpu.CompilerParams(vmem_limit_bytes=SMALL_GRANT),
        name="statistics",
    )(values)


def normalise_kernel(values_ref, *rest):
    stat_refs, rest = rest[:-6], rest[-6:]
    affine_ref, weight_ref, normed_ref, part_ref, held, semaphore = rest
    copy = pltpu.make_async_copy(weight_ref.at[:, : held.shape[1]], held, semaphore)
    copy.start()
    width = values_ref.shape[1]
    stats = [ref[...] for ref in stat_refs]
    mean = sum(one[0:1] for one in stats) / len(stats)
    squares = sum(one[1:2] + width * jnp.square(one[0:1] - mean) for one in stats)
    scale = lax.rsqrt(squares / (width * len(stats)) + EPS)
    row = lax.broadcasted_iota(jnp.int32, (128, mean.shape[1]), 0)
    columns = jnp.where(row == 0, mean, scale).T
    values = values_ref[...].astype(jnp.float32)
    normed = (values - columns[:, 0:1]) * columns[:, 1:2] * affine_ref[0:1] + affine_ref[1:2]
    normed_ref[...] = normed.astype(normed_ref.dtype)
    copy.wait()
    part_ref[...] = jnp.dot(
        normed_ref[...], held[...], preferred_element_type=jnp.float32
    ).astype(part_ref.dtype)


def normalise(values, stats, affine, weight, piece):
    tokens, width = values.shape
    whole = pl.BlockSpec(memory_space=pltpu.VMEM)
    return pl.pallas_call(
        normalise_kernel,
        in_specs=[whole] * (len(stats) + 2) + [pl.BlockSpec(memory_space=pltpu.HBM)],
        out_specs=[whole] * 2,
        out_shape=[
            jax.ShapeDtypeStruct((tokens, width), jnp.bfloat16),
            jax.ShapeDtypeStruct((tokens, piece), jnp.bfloat16),
        ],
        scratch_shapes=[pltpu.VMEM((width, piece), weight.dtype), pltpu.SemaphoreType.DMA],
        compiler_params=pltpu.CompilerParams(vmem_limit_bytes=LARGE_GRANT),
        name="normalise",
    )(values, *stats, affine, weight)


def up_kernel(first, rows_ref, weight_ref, *rest):
    out_refs, (held, semaphores) = rest[:-2], rest[-2:]
    copies = []
    for at in range(len(out_refs)):
        columns = pl.ds((first + at) * held.shape[2], held.shape[2])
        copies.append(
            pltpu.make_async_copy(weight_ref.at[:, columns], held.at[at], semaphores.at[at])
        )
        copies[at].start()
    for at, out_ref in enumerate(out_refs):
        copies[at].wait()
        product = jnp.dot(rows_ref[...], held[at], preferred_element_type=jnp.float32)
        out_ref[...] = product.astype(out_ref.dtype)


def up_pieces(rows, weight, first, count, piece):
    tokens, depth = rows.shape
    whole = pl.BlockSpec(memory_space=pltpu.VMEM)
    held = 2 * depth * piece * count
    moved = 2 * tokens * (depth + piece * count)
    return pl.pallas_call(
        functools.partial(up_kernel, first),
        in_specs=[whole, pl.BlockSpec(memory_space=pltpu.HBM)],
        out_specs=[whole] * count,
        out_shape=[jax.ShapeDtypeStruct((tokens, piece), jnp.bfloat16)] * count,
        scratch_shapes=[
            pltpu.VMEM((count, depth, piece), weight.dtype),
            pltpu.SemaphoreType.DMA((count,)),
        ],
        compiler_params=pltpu.CompilerParams(vmem_limit_bytes=LARGE_GRANT),
        cost_estimate=pl.CostEstimate(
            flops=2 * tokens * depth * piece * count,
            bytes_accessed=held + moved,
            transcendentals=0,
        ),
    )(rows, weight)


def feed_forward_line(residual_in, gain_in, shift_in, up_weight, down_weight):
    place = lax.axis_index("cb")
    at_end = jnp.logical_or(place == 0, place == 3)
    inwards, outwards = [(0, 1), (3, 2)], [(1, 0), (2, 3)]
    piece = up_weight.shape[1] // PIECES
    own, kept = statistics(residual_in)
    stats = gathered(own, "cb")
    affine = jnp.stack([gain_in, shift_in])
    normed, part = normalise(kept, stats, affine, up_weight, piece)
    parts = [part]
    for first, count in GROUPS:
        parts += up_pieces(normed, up_weight, first, count, piece)
    hidden = {}
    branch = None
    for step in range(PIECES + LAG):
        done = step - LAG
        if done < 0:
            sent, pairs = parts[step], inwards
        elif step < PIECES:
            sent = jnp.where(at_end, parts[step], hidden[done])
            pairs = inwards + outwards
        else:
            sent, pairs = hidden[done], outwards
        got = lax.ppermute(sent, "cb", pairs)
        if step < PIECES:
            half = parts[step].astype(jnp.float32) + got.astype(jnp.float32)
            rounded_half = half.astype(jnp.bfloat16)
            other = lax.ppermute(rounded_half, "cb", [(1, 2), (2, 1)])
            hidden[step] = activate(half + other.astype(jnp.float32))
        if done >= 0:
            whole = jnp.where(at_end, got, hidden[done])
            product = jnp.dot(whole, down_weight[done * piece : (done + 1) * piece], preferred_element_type=jnp.float32)
            if done == PIECES - 1:
                return normed, branch, product
            branch = lax.optimization_barrier(product if done == 0 else branch + product)


def feed_forward_any(normed, up_weight, down_weight):
    products = jnp.dot(normed, up_weight, preferred_element_type=jnp.float32)
    share = lax.psum_scatter(products, "cb", scatter_dimension=1, tiled=True)
    hidden = lax.all_gather(activate(share), "cb", axis=1, tiled=True)
    return jnp.dot(hidden, down_weight, preferred_element_type=jnp.float32)


def per_device(residual_in, gain_in, shift_in, up_weight, down_weight, gain_out, shift_out):
    sizes = {axis: lax.axis_size(axis) for axis in ("ra", "cb")}
    if sizes == {"ra": 2, "cb": 4} and up_weight.shape[1] % (128 * PIECES) == 0:
        normed, most, last = feed_forward_line(
            residual_in, gain_in, shift_in, up_weight, down_weight
        )
        swap = functools.partial(lax.ppermute, axis_name="ra", perm=[(0, 1), (1, 0)])
        last = last.astype(jnp.bfloat16)
        total = 2.0**0.25 * normed.astype(jnp.float32) + (most + swap(most))
        total = total + (last.astype(jnp.float32) + swap(last).astype(jnp.float32))
    else:
        normed = layer_norm(residual_in.astype(jnp.float32), gain_in, shift_in)
        normed = normed.astype(jnp.bfloat16)
        branch = lax.psum(feed_forward_any(normed, up_weight, down_weight), "ra")
        total = 2.0**0.25 * normed.astype(jnp.float32) + branch
    return layer_norm(total, gain_out, shift_out).astype(jnp.bfloat16)


def solution(mesh):
    in_specs = (P("dp", "cb"), P("cb"), P("cb"), P("cb", "ra"), P("ra", "cb"), P("cb"), P("cb"))
    out_specs = P("dp", "cb")
    return jax.shard_map(
        per_device, mesh=mesh, in_specs=in_specs, out_specs=out_specs, check_vma=False
    )
```

time: 176 us -> 174 us (0.989)
  matrix products: 25.2 us -> 12.5 us
  Pallas kernels: 0 us -> 12.4 us
  waiting for transfers between devices: 56.7 us -> 54.8 us
    dot_general x32 -> x16, matrix products: 25.2 us -> 12.5 us  [feed_forward_line(): jnp.dot(whole, down_weight[done * piece:(done + 1) * piece], preferred_el...]
    pallas_call x0 -> x5, Pallas kernels: none -> 12.4 us  [the longest x3 10.4 us: up_pieces(): pl.pallas_call(functools.partial(up_kernel, first), in_specs=[whole, pl.B...]
    add x0 -> x14, other arithmetic: none -> 2.41 us  [feed_forward_line(): branch + product]
    convert_element_type x17 -> x16, other arithmetic: 3.13 us -> 1.06 us  [feed_forward_line(): rounded_half = half.astype(jnp.bfloat16)]
    ppermute x42 -> x44, waiting for transfers between devices: 56.7 us -> 54.8 us  [the longest x20 48.5 us: feed_forward_line(): got = lax.ppermute(sent, 'cb', pairs)]
    ppermute x42 -> x44, starting transfers between devices: 82.6 us -> 82.8 us  [the longest x20 59.5 us: feed_forward_line(): got = lax.ppermute(sent, 'cb', pairs)]
  transfers between devices with their start and end apart: 42 -> 44, of which waited for: 24 -> 19; matrix products, arithmetic and copies ran while one was open for 6% -> 11% of each run, Pallas kernels for 0% -> 5%
where the time goes in v2:
time: 174 us; the launch traced here: 173 us
  starting transfers between devices  82.8 us (48%)
  waiting for transfers between devices  54.8 us (31%)
  matrix products  12.5 us (7%)
  Pallas kernels  12.4 us (7%)
  other arithmetic  8.51 us (5%)
    ppermute x20, starting transfers between devices, feed_forward_line(): got = lax.ppermute(sent, 'cb', pairs)  59.5 us
    ppermute x20, waiting for transfers between devices, feed_forward_line(): got = lax.ppermute(sent, 'cb', pairs)  48.5 us
    dot_general x16, matrix products, feed_forward_line(): jnp.dot(whole, down_weight[done * piece:(done + 1) * piece], preferred_el...  12.5 us
    ppermute x6, starting transfers between devices, gathered(): return [values] + [lax.ppermute(values, axis, pairs) for pairs in shifts]  11.4 us
    ppermute x16, starting transfers between devices, feed_forward_line(): other = lax.ppermute(rounded_half, 'cb', [(1, 2), (2, 1)])  11.3 us
    pallas_call x3, Pallas kernels, up_pieces(): pl.pallas_call(functools.partial(up_kernel, first), in_specs=[whole, pl.B...  10.4 us
    ppermute x6, waiting for transfers between devices, gathered(): return [values] + [lax.ppermute(values, axis, pairs) for pairs in shifts]  3.79 us
  transfers between devices with their start and end apart: 44, of which 19 were waited for; matrix products, arithmetic and copies ran while one was open for 11% of the time, Pallas kernels for 5%

profile of v2, /device:TPU:0, one launch (start us, length us, event | category | flops | bytes accessed | tf_op | source)
XLA Modules:
  0.0 172.9 jit_solution(7734960719303810993)
XLA Ops:
  1.4 3.1 %collective-permute-start = (f32[8,256]{1,0:T(8,128)S(1)}, f32[8,256]{1,0:T(8,128)S(1)}, u32[]{:S(2)}, u32[]{:S(2)}) collective-permute-start(f32[8,256]{1,0:T(8,128)S(1)} %get-tuple-element.25.rest_0_), channel_id=1, source_target_pairs={{0,4},{4,8},{8,12},{12,0},{1,5},{5,9},{9,13},{13,1},{2,6},{6,10},{... | collective-permute-start | bytes 24584 | tf_op jit(solution)/shard_map/ppermute | solution.py:24
  4.5 2.6 %collective-permute-start.1 = (f32[8,256]{1,0:T(8,128)S(1)}, f32[8,256]{1,0:T(8,128)S(1)}, u32[]{:S(2)}, u32[]{:S(2)}) collective-permute-start(f32[8,256]{1,0:T(8,128)S(1)} %get-tuple-element.25.rest_0_), channel_id=1, source_target_pairs={{0,8},{4,12},{8,0},{12,4},{1,9},{5,13},{9,1},{13,5},{2,10},{6,14},... | collective-permute-start | bytes 24584 | tf_op jit(solution)/shard_map/ppermute | solution.py:24
  12.4 2.6 %shard_map.74 = (bf16[256,512]{1,0:T(8,128)(2,1)S(1)}, bf16[256,512]{1,0:T(8,128)(2,1)S(1)}, bf16[256,512]{1,0:T(8,128)(2,1)S(1)}) custom-call(bf16[256,1024]{1,0:T(8,128)(2,1)S(1)} %get-tuple-element.26.rows_ref, bf16[1024,8192]{1,0:T(8,128)(2,1)} %weight_ref.5), custom_call_target="tpu_custom_call" | custom-call | flops 805306368 | bytes 4456448 | tf_op jit(solution)/shard_map/pallas_call | solution.py:136
  18.3 3.9 %shard_map.75 = (bf16[256,512]{1,0:T(8,128)(2,1)S(1)}, bf16[256,512]{1,0:T(8,128)(2,1)S(1)}, bf16[256,512]{1,0:T(8,128)(2,1)S(1)}, bf16[256,512]{1,0:T(8,128)(2,...) custom-call(bf16[256,1024]{1,0:T(8,128)(2,1)S(1)} %get-tuple-element.26.rows_ref, ...), custom_call_target="tpu_custom_call" | custom-call | flops 1610612736 | bytes 8388608 | tf_op jit(solution)/shard_map/pallas_call | solution.py:136
  22.2 3.9 %shard_map.73 = (bf16[256,512]{1,0:T(8,128)(2,1)S(1)}, bf16[256,512]{1,0:T(8,128)(2,1)S(1)}, bf16[256,512]{1,0:T(8,128)(2,1)S(1)}, bf16[256,512]{1,0:T(8,128)(2,...) custom-call(bf16[256,1024]{1,0:T(8,128)(2,1)S(1)} %get-tuple-element.26.rows_ref, ...), custom_call_target="tpu_custom_call" | custom-call | flops 1610612736 | bytes 8388608 | tf_op jit(solution)/shard_map/pallas_call | solution.py:136
  30.3 3.8 %collective-permute-done.6 = bf16[256,512]{1,0:T(8,128)(2,1)S(1)} collective-permute-done((bf16[256,512]{1,0:T(8,128)(2,1)S(1)}, bf16[256,512]{1,0:T(8,128)(2,1)S(1)}, u32[]{:S(2)}, u32[]{:S(2)}) %collective-permute-start.6) | collective-permute-done | bytes 262176 | tf_op jit(solution)/shard_map/ppermute | solution.py:177
  34.8 3.1 %collective-permute-done.9 = bf16[256,512]{1,0:T(8,128)(2,1)S(1)} collective-permute-done((bf16[256,512]{1,0:T(8,128)(2,1)S(1)}, bf16[256,512]{1,0:T(8,128)(2,1)S(1)}, u32[]{:S(2)}, u32[]{:S(2)}) %collective-permute-start.9) | collective-permute-done | bytes 262176 | tf_op jit(solution)/shard_map/ppermute | solution.py:177
  38.9 5.3 %collective-permute-start.14 = (bf16[256,512]{1,0:T(8,128)(2,1)S(1)}, bf16[256,512]{1,0:T(8,128)(2,1)S(1)}, u32[]{:S(2)}, u32[]{:S(2)}) collective-permute-start(bf16[256,512]{1,0:T(8,128)(2,1)S(1)} %broadcast_select_fusion.8), channel_id=1, source_target_pairs={{0,4},{12,8},{4,0},{8,12},{1,5},{13,9},{5,1},{9,13},{2,6},{14,10},... | collective-permute-start | bytes 786440 | tf_op jit(solution)/shard_map/ppermute | solution.py:177
  45.2 5.4 %collective-permute-start.8 = (bf16[256,512]{1,0:T(8,128)(2,1)S(1)}, bf16[256,512]{1,0:T(8,128)(2,1)S(1)}, u32[]{:S(2)}, u32[]{:S(2)}) collective-permute-start(bf16[256,512]{1,0:T(8,128)(2,1)S(1)} %broadcast_select_fusion.10), channel_id=1, source_target_pairs={{0,4},{12,8},{4,0},{8,12},{1,5},{13,9},{5,1},{9,13},{2,6},{14,10},... | collective-permute-start | bytes 786440 | tf_op jit(solution)/shard_map/ppermute | solution.py:177
  50.8 2.9 %collective-permute-start.11 = (bf16[256,512]{1,0:T(8,128)(2,1)S(1)}, bf16[256,512]{1,0:T(8,128)(2,1)S(1)}, u32[]{:S(2)}, u32[]{:S(2)}) collective-permute-start(bf16[256,512]{1,0:T(8,128)(2,1)S(1)} %broadcast_select_fusion.9), channel_id=1, source_target_pairs={{0,4},{12,8},{4,0},{8,12},{1,5},{13,9},{5,1},{9,13},{2,6},{14,10},... | collective-permute-start | bytes 786440 | tf_op jit(solution)/shard_map/ppermute | solution.py:177
  54.5 2.5 %collective-permute-done.5 = bf16[256,512]{1,0:T(8,128)(2,1)S(1)} collective-permute-done((bf16[256,512]{1,0:T(8,128)(2,1)S(1)}, bf16[256,512]{1,0:T(8,128)(2,1)S(1)}, u32[]{:S(2)}, u32[]{:S(2)}) %collective-permute-start.5) | collective-permute-done | bytes 262176 | tf_op jit(solution)/shard_map/ppermute | solution.py:177
  58.7 3.9 %collective-permute-done.8 = bf16[256,512]{1,0:T(8,128)(2,1)S(1)} collective-permute-done((bf16[256,512]{1,0:T(8,128)(2,1)S(1)}, bf16[256,512]{1,0:T(8,128)(2,1)S(1)}, u32[]{:S(2)}, u32[]{:S(2)}) %collective-permute-start.8) | collective-permute-done | bytes 262176 | tf_op jit(solution)/shard_map/ppermute | solution.py:177
  72.2 8.0 %collective-permute-start.22 = (bf16[256,512]{1,0:T(8,128)(2,1)S(1)}, bf16[256,512]{1,0:T(8,128)(2,1)S(1)}, u32[]{:S(2)}, u32[]{:S(2)}) collective-permute-start(bf16[256,512]{1,0:T(8,128)(2,1)S(1)} %broadcast_select_fusion.4), channel_id=1, source_target_pairs={{0,4},{12,8},{4,0},{8,12},{1,5},{13,9},{5,1},{9,13},{2,6},{14,10},... | collective-permute-start | bytes 786440 | tf_op jit(solution)/shard_map/ppermute | solution.py:177
  80.4 2.5 %collective-permute-start.16 = (bf16[256,512]{1,0:T(8,128)(2,1)S(1)}, bf16[256,512]{1,0:T(8,128)(2,1)S(1)}, u32[]{:S(2)}, u32[]{:S(2)}) collective-permute-start(bf16[256,512]{1,0:T(8,128)(2,1)S(1)} %broadcast_select_fusion.7), channel_id=1, source_target_pairs={{0,4},{12,8},{4,0},{8,12},{1,5},{13,9},{5,1},{9,13},{2,6},{14,10},... | collective-permute-start | bytes 786440 | tf_op jit(solution)/shard_map/ppermute | solution.py:177
  83.1 4.5 %collective-permute-start.18 = (bf16[256,512]{1,0:T(8,128)(2,1)S(1)}, bf16[256,512]{1,0:T(8,128)(2,1)S(1)}, u32[]{:S(2)}, u32[]{:S(2)}) collective-permute-start(bf16[256,512]{1,0:T(8,128)(2,1)S(1)} %broadcast_select_fusion.6), channel_id=1, source_target_pairs={{0,4},{12,8},{4,0},{8,12},{1,5},{13,9},{5,1},{9,13},{2,6},{14,10},... | collective-permute-start | bytes 786440 | tf_op jit(solution)/shard_map/ppermute | solution.py:177
  87.7 2.6 %collective-permute-start.20 = (bf16[256,512]{1,0:T(8,128)(2,1)S(1)}, bf16[256,512]{1,0:T(8,128)(2,1)S(1)}, u32[]{:S(2)}, u32[]{:S(2)}) collective-permute-start(bf16[256,512]{1,0:T(8,128)(2,1)S(1)} %broadcast_select_fusion.5), channel_id=1, source_target_pairs={{0,4},{12,8},{4,0},{8,12},{1,5},{13,9},{5,1},{9,13},{2,6},{14,10},... | collective-permute-start | bytes 786440 | tf_op jit(solution)/shard_map/ppermute | solution.py:177
  93.7 3.4 %collective-permute-done.18 = bf16[256,512]{1,0:T(8,128)(2,1)S(1)} collective-permute-done((bf16[256,512]{1,0:T(8,128)(2,1)S(1)}, bf16[256,512]{1,0:T(8,128)(2,1)S(1)}, u32[]{:S(2)}, u32[]{:S(2)}) %collective-permute-start.18) | collective-permute-done | bytes 262176 | tf_op jit(solution)/shard_map/ppermute | solution.py:177
  103.7 9.1 %collective-permute-start.30 = (bf16[256,512]{1,0:T(8,128)(2,1)S(1)}, bf16[256,512]{1,0:T(8,128)(2,1)S(1)}, u32[]{:S(2)}, u32[]{:S(2)}) collective-permute-start(bf16[256,512]{1,0:T(8,128)(2,1)S(1)} %broadcast_select_fusion), channel_id=1, source_target_pairs={{0,4},{12,8},{4,0},{8,12},{1,5},{13,9},{5,1},{9,13},{2,6},{14,10},... | collective-permute-start | bytes 786440 | tf_op jit(solution)/shard_map/ppermute | solution.py:177
  114.5 3.2 %collective-permute-start.26 = (bf16[256,512]{1,0:T(8,128)(2,1)S(1)}, bf16[256,512]{1,0:T(8,128)(2,1)S(1)}, u32[]{:S(2)}, u32[]{:S(2)}) collective-permute-start(bf16[256,512]{1,0:T(8,128)(2,1)S(1)} %broadcast_select_fusion.2), channel_id=1, source_target_pairs={{0,4},{12,8},{4,0},{8,12},{1,5},{13,9},{5,1},{9,13},{2,6},{14,10},... | collective-permute-start | bytes 786440 | tf_op jit(solution)/shard_map/ppermute | solution.py:177
  117.9 2.8 %collective-permute-start.28 = (bf16[256,512]{1,0:T(8,128)(2,1)S(1)}, bf16[256,512]{1,0:T(8,128)(2,1)S(1)}, u32[]{:S(2)}, u32[]{:S(2)}) collective-permute-start(bf16[256,512]{1,0:T(8,128)(2,1)S(1)} %broadcast_select_fusion.1), channel_id=1, source_target_pairs={{0,4},{12,8},{4,0},{8,12},{1,5},{13,9},{5,1},{9,13},{2,6},{14,10},... | collective-permute-start | bytes 786440 | tf_op jit(solution)/shard_map/ppermute | solution.py:177
  121.4 3.7 %collective-permute-done.24 = bf16[256,512]{1,0:T(8,128)(2,1)S(1)} collective-permute-done((bf16[256,512]{1,0:T(8,128)(2,1)S(1)}, bf16[256,512]{1,0:T(8,128)(2,1)S(1)}, u32[]{:S(2)}, u32[]{:S(2)}) %collective-permute-start.24) | collective-permute-done | bytes 262176 | tf_op jit(solution)/shard_map/ppermute | solution.py:177
  140.1 14.2 %collective-permute-done.32 = bf16[256,512]{1,0:T(8,128)(2,1)S(1)} collective-permute-done((bf16[256,512]{1,0:T(8,128)(2,1)S(1)}, bf16[256,512]{1,0:T(8,128)(2,1)S(1)}, u32[]{:S(2)}, u32[]{:S(2)}) %collective-permute-start.32) | collective-permute-done | bytes 262176 | tf_op jit(solution)/shard_map/ppermute | solution.py:177
  162.0 2.4 %collective-permute-done.40 = bf16[256,1024]{1,0:T(8,128)(2,1)S(1)} collective-permute-done((bf16[256,1024]{1,0:T(8,128)(2,1)S(1)}, bf16[256,1024]{1,0:T(8,128)(2,1)S(1)}, u32[]{:S(2)}, u32[]{:S(2)}) %collective-permute-start.40) | collective-permute-done | bytes 524320 | tf_op jit(solution)/shard_map/ppermute | solution.py:207
  165.6 2.5 %collective-permute-start.41 = (f32[2,256]{1,0:T(2,128)S(1)}, f32[2,256]{1,0:T(2,128)S(1)}, u32[]{:S(2)}, u32[]{:S(2)}) collective-permute-start(f32[2,256]{1,0:T(2,128)S(1)} %get-tuple-element.48), channel_id=1, source_target_pairs={{0,4},{4,8},{8,12},{12,0},{1,5},{5,9},{9,13},{13,1},{2,6},{6,10},{... | collective-permute-start | bytes 6152 | tf_op jit(solution)/shard_map/ppermute | solution.py:24
  (161 shorter events, 70.2 us)
Async XLA Ops:
  15.0 13.8 %collective-permute-start.12 = (bf16[256,512]{1,0:T(8,128)(2,1)S(1)}, bf16[256,512]{1,0:T(8,128)(2,1)S(1)}, u32[]{:S(2)}, u32[]{:S(2)}) collective-permute-start(bf16[256,512]{1,0:T(8,128)(2,1)S(1)} %get-tuple-element.34), channel_id=1, source_target_pairs={{0,4},{12,8},{1,5},{13,9},{2,6},{14,10},{3,7},{15,11},{16,20},{28,... | collective-permute-start | bytes 786440 | tf_op jit(solution)/shard_map/ppermute | solution.py:177
  17.0 12.5 %collective-permute-start.3 = (bf16[256,512]{1,0:T(8,128)(2,1)S(1)}, bf16[256,512]{1,0:T(8,128)(2,1)S(1)}, u32[]{:S(2)}, u32[]{:S(2)}) collective-permute-start(bf16[256,512]{1,0:T(8,128)(2,1)S(1)} %get-tuple-element.28), channel_id=1, source_target_pairs={{0,4},{12,8},{1,5},{13,9},{2,6},{14,10},{3,7},{15,11},{16,20},{28,... | collective-permute-start | bytes 786440 | tf_op jit(solution)/shard_map/ppermute | solution.py:177
  29.6 14.6 %collective-permute-start.4 = (bf16[256,512]{1,0:T(8,128)(2,1)S(1)}, bf16[256,512]{1,0:T(8,128)(2,1)S(1)}, u32[]{:S(2)}, u32[]{:S(2)}) collective-permute-start(bf16[256,512]{1,0:T(8,128)(2,1)S(1)} %fusion.31), channel_id=1, source_target_pairs={{4,8},{8,4},{5,9},{9,5},{6,10},{10,6},{7,11},{11,7},{20,24},{24,20... | collective-permute-start | bytes 786440 | tf_op jit(solution)/shard_map/ppermute | solution.py:181
  38.0 12.7 %collective-permute-start.10 = (bf16[256,512]{1,0:T(8,128)(2,1)S(1)}, bf16[256,512]{1,0:T(8,128)(2,1)S(1)}, u32[]{:S(2)}, u32[]{:S(2)}) collective-permute-start(bf16[256,512]{1,0:T(8,128)(2,1)S(1)} %fusion.33), channel_id=1, source_target_pairs={{4,8},{8,4},{5,9},{9,5},{6,10},{10,6},{7,11},{11,7},{20,24},{24,20... | collective-permute-start | bytes 786440 | tf_op jit(solution)/shard_map/ppermute | solution.py:181
  38.9 14.9 %collective-permute-start.14 = (bf16[256,512]{1,0:T(8,128)(2,1)S(1)}, bf16[256,512]{1,0:T(8,128)(2,1)S(1)}, u32[]{:S(2)}, u32[]{:S(2)}) collective-permute-start(bf16[256,512]{1,0:T(8,128)(2,1)S(1)} %broadcast_select_fusion.8), channel_id=1, source_target_pairs={{0,4},{12,8},{4,0},{8,12},{1,5},{13,9},{5,1},{9,13},{2,6},{14,10},... | collective-permute-start | bytes 786440 | tf_op jit(solution)/shard_map/ppermute | solution.py:177
  44.4 12.6 %collective-permute-start.5 = (bf16[256,512]{1,0:T(8,128)(2,1)S(1)}, bf16[256,512]{1,0:T(8,128)(2,1)S(1)}, u32[]{:S(2)}, u32[]{:S(2)}) collective-permute-start(bf16[256,512]{1,0:T(8,128)(2,1)S(1)} %broadcast_select_fusion.11), channel_id=1, source_target_pairs={{0,4},{12,8},{4,0},{8,12},{1,5},{13,9},{5,1},{9,13},{2,6},{14,10},... | collective-permute-start | bytes 786440 | tf_op jit(solution)/shard_map/ppermute | solution.py:177
  45.2 17.4 %collective-permute-start.8 = (bf16[256,512]{1,0:T(8,128)(2,1)S(1)}, bf16[256,512]{1,0:T(8,128)(2,1)S(1)}, u32[]{:S(2)}, u32[]{:S(2)}) collective-permute-start(bf16[256,512]{1,0:T(8,128)(2,1)S(1)} %broadcast_select_fusion.10), channel_id=1, source_target_pairs={{0,4},{12,8},{4,0},{8,12},{1,5},{13,9},{5,1},{9,13},{2,6},{14,10},... | collective-permute-start | bytes 786440 | tf_op jit(solution)/shard_map/ppermute | solution.py:177
  50.8 14.7 %collective-permute-start.11 = (bf16[256,512]{1,0:T(8,128)(2,1)S(1)}, bf16[256,512]{1,0:T(8,128)(2,1)S(1)}, u32[]{:S(2)}, u32[]{:S(2)}) collective-permute-start(bf16[256,512]{1,0:T(8,128)(2,1)S(1)} %broadcast_select_fusion.9), channel_id=1, source_target_pairs={{0,4},{12,8},{4,0},{8,12},{1,5},{13,9},{5,1},{9,13},{2,6},{14,10},... | collective-permute-start | bytes 786440 | tf_op jit(solution)/shard_map/ppermute | solution.py:177
  53.8 18.2 %collective-permute-start.21 = (bf16[256,512]{1,0:T(8,128)(2,1)S(1)}, bf16[256,512]{1,0:T(8,128)(2,1)S(1)}, u32[]{:S(2)}, u32[]{:S(2)}) collective-permute-start(bf16[256,512]{1,0:T(8,128)(2,1)S(1)} %fusion.38), channel_id=1, source_target_pairs={{4,8},{8,4},{5,9},{9,5},{6,10},{10,6},{7,11},{11,7},{20,24},{24,20... | collective-permute-start | bytes 786440 | tf_op jit(solution)/shard_map/ppermute | solution.py:181
  70.5 12.4 %collective-permute-start.17 = (bf16[256,512]{1,0:T(8,128)(2,1)S(1)}, bf16[256,512]{1,0:T(8,128)(2,1)S(1)}, u32[]{:S(2)}, u32[]{:S(2)}) collective-permute-start(bf16[256,512]{1,0:T(8,128)(2,1)S(1)} %fusion.36), channel_id=1, source_target_pairs={{4,8},{8,4},{5,9},{9,5},{6,10},{10,6},{7,11},{11,7},{20,24},{24,20... | collective-permute-start | bytes 786440 | tf_op jit(solution)/shard_map/ppermute | solution.py:181
  71.4 16.2 %collective-permute-start.19 = (bf16[256,512]{1,0:T(8,128)(2,1)S(1)}, bf16[256,512]{1,0:T(8,128)(2,1)S(1)}, u32[]{:S(2)}, u32[]{:S(2)}) collective-permute-start(bf16[256,512]{1,0:T(8,128)(2,1)S(1)} %fusion.37), channel_id=1, source_target_pairs={{4,8},{8,4},{5,9},{9,5},{6,10},{10,6},{7,11},{11,7},{20,24},{24,20... | collective-permute-start | bytes 786440 | tf_op jit(solution)/shard_map/ppermute | solution.py:181
  72.2 18.1 %collective-permute-start.22 = (bf16[256,512]{1,0:T(8,128)(2,1)S(1)}, bf16[256,512]{1,0:T(8,128)(2,1)S(1)}, u32[]{:S(2)}, u32[]{:S(2)}) collective-permute-start(bf16[256,512]{1,0:T(8,128)(2,1)S(1)} %broadcast_select_fusion.4), channel_id=1, source_target_pairs={{0,4},{12,8},{4,0},{8,12},{1,5},{13,9},{5,1},{9,13},{2,6},{14,10},... | collective-permute-start | bytes 786440 | tf_op jit(solution)/shard_map/ppermute | solution.py:177
  80.4 12.6 %collective-permute-start.16 = (bf16[256,512]{1,0:T(8,128)(2,1)S(1)}, bf16[256,512]{1,0:T(8,128)(2,1)S(1)}, u32[]{:S(2)}, u32[]{:S(2)}) collective-permute-start(bf16[256,512]{1,0:T(8,128)(2,1)S(1)} %broadcast_select_fusion.7), channel_id=1, source_target_pairs={{0,4},{12,8},{4,0},{8,12},{1,5},{13,9},{5,1},{9,13},{2,6},{14,10},... | collective-permute-start | bytes 786440 | tf_op jit(solution)/shard_map/ppermute | solution.py:177
  83.1 14.0 %collective-permute-start.18 = (bf16[256,512]{1,0:T(8,128)(2,1)S(1)}, bf16[256,512]{1,0:T(8,128)(2,1)S(1)}, u32[]{:S(2)}, u32[]{:S(2)}) collective-permute-start(bf16[256,512]{1,0:T(8,128)(2,1)S(1)} %broadcast_select_fusion.6), channel_id=1, source_target_pairs={{0,4},{12,8},{4,0},{8,12},{1,5},{13,9},{5,1},{9,13},{2,6},{14,10},... | collective-permute-start | bytes 786440 | tf_op jit(solution)/shard_map/ppermute | solution.py:177
  90.4 13.1 %collective-permute-start.29 = (bf16[256,512]{1,0:T(8,128)(2,1)S(1)}, bf16[256,512]{1,0:T(8,128)(2,1)S(1)}, u32[]{:S(2)}, u32[]{:S(2)}) collective-permute-start(bf16[256,512]{1,0:T(8,128)(2,1)S(1)} %fusion.42), channel_id=1, source_target_pairs={{4,8},{8,4},{5,9},{9,5},{6,10},{10,6},{7,11},{11,7},{20,24},{24,20... | collective-permute-start | bytes 786440 | tf_op jit(solution)/shard_map/ppermute | solution.py:181
  102.8 14.9 %collective-permute-start.27 = (bf16[256,512]{1,0:T(8,128)(2,1)S(1)}, bf16[256,512]{1,0:T(8,128)(2,1)S(1)}, u32[]{:S(2)}, u32[]{:S(2)}) collective-permute-start(bf16[256,512]{1,0:T(8,128)(2,1)S(1)} %fusion.41), channel_id=1, source_target_pairs={{4,8},{8,4},{5,9},{9,5},{6,10},{10,6},{7,11},{11,7},{20,24},{24,20... | collective-permute-start | bytes 786440 | tf_op jit(solution)/shard_map/ppermute | solution.py:181
  103.7 17.0 %collective-permute-start.30 = (bf16[256,512]{1,0:T(8,128)(2,1)S(1)}, bf16[256,512]{1,0:T(8,128)(2,1)S(1)}, u32[]{:S(2)}, u32[]{:S(2)}) collective-permute-start(bf16[256,512]{1,0:T(8,128)(2,1)S(1)} %broadcast_select_fusion), channel_id=1, source_target_pairs={{0,4},{12,8},{4,0},{8,12},{1,5},{13,9},{5,1},{9,13},{2,6},{14,10},... | collective-permute-start | bytes 786440 | tf_op jit(solution)/shard_map/ppermute | solution.py:177
  114.5 13.4 %collective-permute-start.26 = (bf16[256,512]{1,0:T(8,128)(2,1)S(1)}, bf16[256,512]{1,0:T(8,128)(2,1)S(1)}, u32[]{:S(2)}, u32[]{:S(2)}) collective-permute-start(bf16[256,512]{1,0:T(8,128)(2,1)S(1)} %broadcast_select_fusion.2), channel_id=1, source_target_pairs={{0,4},{12,8},{4,0},{8,12},{1,5},{13,9},{5,1},{9,13},{2,6},{14,10},... | collective-permute-start | bytes 786440 | tf_op jit(solution)/shard_map/ppermute | solution.py:177
  117.9 12.8 %collective-permute-start.28 = (bf16[256,512]{1,0:T(8,128)(2,1)S(1)}, bf16[256,512]{1,0:T(8,128)(2,1)S(1)}, u32[]{:S(2)}, u32[]{:S(2)}) collective-permute-start(bf16[256,512]{1,0:T(8,128)(2,1)S(1)} %broadcast_select_fusion.1), channel_id=1, source_target_pairs={{0,4},{12,8},{4,0},{8,12},{1,5},{13,9},{5,1},{9,13},{2,6},{14,10},... | collective-permute-start | bytes 786440 | tf_op jit(solution)/shard_map/ppermute | solution.py:177
  120.7 13.6 %collective-permute-start.38 = (bf16[256,512]{1,0:T(8,128)(2,1)S(1)}, bf16[256,512]{1,0:T(8,128)(2,1)S(1)}, u32[]{:S(2)}, u32[]{:S(2)}) collective-permute-start(bf16[256,512]{1,0:T(8,128)(2,1)S(1)} %fusion.46), channel_id=1, source_target_pairs={{4,8},{8,4},{5,9},{9,5},{6,10},{10,6},{7,11},{11,7},{20,24},{24,20... | collective-permute-start | bytes 786440 | tf_op jit(solution)/shard_map/ppermute | solution.py:181
  134.5 26.5 %collective-permute-start.39 = (bf16[256,512]{1,0:T(8,128)(2,1)S(1)}, bf16[256,512]{1,0:T(8,128)(2,1)S(1)}, u32[]{:S(2)}, u32[]{:S(2)}) collective-permute-start(bf16[256,512]{1,0:T(8,128)(2,1)S(1)} %multiply_convert_fusion), channel_id=1, source_target_pairs={{4,0},{8,12},{5,1},{9,13},{6,2},{10,14},{7,3},{11,15},{20,16},{24,... | collective-permute-start | bytes 786440 | tf_op jit(solution)/shard_map/ppermute | solution.py:177
  135.9 18.4 %collective-permute-start.32 = (bf16[256,512]{1,0:T(8,128)(2,1)S(1)}, bf16[256,512]{1,0:T(8,128)(2,1)S(1)}, u32[]{:S(2)}, u32[]{:S(2)}) collective-permute-start(bf16[256,512]{1,0:T(8,128)(2,1)S(1)} %multiply_convert_fusion.3), channel_id=1, source_target_pairs={{4,0},{8,12},{5,1},{9,13},{6,2},{10,14},{7,3},{11,15},{20,16},{24,... | collective-permute-start | bytes 786440 | tf_op jit(solution)/shard_map/ppermute | solution.py:177
  137.4 19.8 %collective-permute-start.34 = (bf16[256,512]{1,0:T(8,128)(2,1)S(1)}, bf16[256,512]{1,0:T(8,128)(2,1)S(1)}, u32[]{:S(2)}, u32[]{:S(2)}) collective-permute-start(bf16[256,512]{1,0:T(8,128)(2,1)S(1)} %multiply_convert_fusion.2), channel_id=1, source_target_pairs={{4,0},{8,12},{5,1},{9,13},{6,2},{10,14},{7,3},{11,15},{20,16},{24,... | collective-permute-start | bytes 786440 | tf_op jit(solution)/shard_map/ppermute | solution.py:177
  138.8 21.2 %collective-permute-start.36 = (bf16[256,512]{1,0:T(8,128)(2,1)S(1)}, bf16[256,512]{1,0:T(8,128)(2,1)S(1)}, u32[]{:S(2)}, u32[]{:S(2)}) collective-permute-start(bf16[256,512]{1,0:T(8,128)(2,1)S(1)} %multiply_convert_fusion.1), channel_id=1, source_target_pairs={{4,0},{8,12},{5,1},{9,13},{6,2},{10,14},{7,3},{11,15},{20,16},{24,... | collective-permute-start | bytes 786440 | tf_op jit(solution)/shard_map/ppermute | solution.py:177
  (27 other events, 359.4 us)
